TPU v7x, 32 devices: a whole 2x2x4 slice. The times are simulated.
32 devices in a mesh: sp: 8 (over z, y), dp: 4 (over x, core).
Axes of the slice: x: 2, y: 2, z: 4, core: 2. Of those that a mesh axis runs over, the one named last changes fastest.
Arguments:
- query_nope: bfloat16 [4, 2048, 16, 128], P('dp', 'sp'), may hold values from -6 to 6
- query_rope: bfloat16 [4, 2048, 16, 64], P('dp', 'sp'), may hold values from -160 to 160
- latent: bfloat16 [4, 2048, 256], P('dp', 'sp'), may hold values from -6 to 6
- key_rope: bfloat16 [4, 2048, 64], P('dp', 'sp'), may hold values from -4 to 4
- resid: bfloat16 [4, 2048, 2048], P('dp', 'sp'), may hold values from -6 to 6
- latent_gain: float32 [256], replicated, may hold values from 0.1 to 1.9
- key_up: bfloat16 [256, 2048], P(None, 'sp'), may hold values from -0.375 to 0.375
- value_up: bfloat16 [256, 2048], P(None, 'sp'), may hold values from -0.375 to 0.375
- out_proj: bfloat16 [2048, 2048], P('sp', 'dp'), may hold values from -0.125 to 0.125
- norm_gain: float32 [2048], replicated, may hold values from 0.1 to 1.9
- expert_gate: bfloat16 [8, 2048, 1024], P('sp'), may hold values from -0.125 to 0.125
- expert_up: bfloat16 [8, 2048, 1024], P('sp'), may hold values from -0.125 to 0.125
- expert_down: bfloat16 [8, 1024, 2048], P('sp'), may hold values from -0.1875 to 0.1875
- routes: int32 [4, 2048, 2], P('dp', 'sp'), may hold values from 0 to 7, all different within a row; in each aligned block of 256 rows (0 to 255, 256 to 511, ..., all dimensions but the last counted through in order) at most 128 rows name the same one
- route_weight: float32 [4, 2048, 2], P('dp', 'sp'), may hold values from 0.2 to 1
Outputs:
- mixed: bfloat16 [4, 2048, 2048], P('dp', 'sp')
Inputs may be any that keep to these rules, and one draw needn't show every extreme that they name: `routes`: each token names two different experts. Among the tokens of one device no expert is named more than 128 times, and in every draw some expert is named exactly 128 times by some device's tokens.
All inputs are finite; a program needn't handle non-finite values.
Results may differ from a plain program's by a relative error of at most 0.0075.
Values may be sent and summed in bfloat16 or wider, within the bound.
No kernel may reach another device: no remote copies, remote signals or barrier semaphores. Data moves between devices by JAX's collectives and lax.ppermute only.
A program may use at most 128 MiB of HBM per device.

v0:
```python
import jax
import jax.numpy as jnp
from jax import lax
from jax.sharding import PartitionSpec as P

epsilon = 1e-06
rope_base = 10000.0
masked_score = -1e30


def rotate(values, positions):
    half_width = values.shape[-1] // 2
    frequency = rope_base ** (-jnp.arange(half_width, dtype=jnp.float32) / half_width)
    angles = positions.astype(jnp.float32)[:, None] * frequency[None, :]
    cosine = jnp.cos(angles)
    sine_part = jnp.sin(angles)
    if values.ndim == 3:
        cosine = cosine[:, None, :]
        sine_part = sine_part[:, None, :]
    floats = values.astype(jnp.float32)
    first_half = floats[..., :half_width]
    second_half = floats[..., half_width:]
    turned = jnp.concatenate(
        [
            first_half * cosine - second_half * sine_part,
            second_half * cosine + first_half * sine_part,
        ],
        axis=-1,
    )
    return turned.astype(jnp.bfloat16)


def rms_scaled(values, gain):
    floats = values.astype(jnp.float32)
    return floats * lax.rsqrt(jnp.mean(floats * floats, axis=-1, keepdims=True) + epsilon) * gain


def assign_slots(route_block, experts_all, capacity):
    flat_routes = route_block.reshape(-1)
    onehot = (flat_routes[:, None] == jnp.arange(experts_all, dtype=jnp.int32)[None, :]).astype(
        jnp.int32
    )
    earlier = jnp.cumsum(onehot, axis=0) - onehot
    placed = jnp.sum(earlier * onehot, axis=1)
    return flat_routes * capacity + placed


def fill_slots(rows, slot_ids, experts_all, capacity):
    pairs = slot_ids.shape[0]
    matches = jnp.arange(experts_all * capacity, dtype=jnp.int32)[:, None] == slot_ids[None, :]
    source = (
        jnp.sum(jnp.where(matches, jnp.arange(pairs, dtype=jnp.int32)[None, :], 0), axis=1) // 2
    )
    filled = jnp.any(matches, axis=1)
    picked = jnp.take(rows, source, axis=0)
    chosen = jnp.where(filled[:, None], picked, jnp.zeros_like(picked))
    return chosen.reshape(experts_all, capacity, rows.shape[-1])


def combine_slots(returned, slot_ids, weights):
    flat_back = returned.reshape(-1, returned.shape[-1])
    picked = (
        jnp.take(flat_back, slot_ids, axis=0).astype(jnp.float32).reshape(weights.shape[0], 2, -1)
    )
    return jnp.sum(weights[:, :, None] * picked, axis=1)


def shards(
    query_nope,
    query_rope,
    latent,
    key_rope,
    resid,
    latent_gain,
    key_up,
    value_up,
    out_proj,
    norm_gain,
    expert_gate,
    expert_up,
    expert_down,
    routes,
    route_weight,
):
    tokens_here = latent.shape[1]
    sp_count = lax.axis_size("sp")
    length = tokens_here * sp_count
    block = min(512, length)
    blocks = length // block
    local_pos = lax.axis_index("sp") * tokens_here + jnp.arange(tokens_here, dtype=jnp.int32)
    latent_normed = rms_scaled(latent[0], latent_gain).astype(jnp.bfloat16)
    key_turned = rotate(key_rope[0], local_pos)
    query_turned = rotate(query_rope[0], local_pos)
    all_latent, all_keyturn = (
        lax.all_gather(latent_normed, "sp", axis=0, tiled=True),
        lax.all_gather(key_turned, "sp", axis=0, tiled=True),
    )
    query_plain, query_turn = (
        lax.all_to_all(query_nope[0], "sp", split_axis=1, concat_axis=0, tiled=True),
        lax.all_to_all(query_turned, "sp", split_axis=1, concat_axis=0, tiled=True),
    )
    heads_here = query_plain.shape[1]
    key_plain = (
        jnp.dot(all_latent, key_up, preferred_element_type=jnp.float32)
        .astype(jnp.bfloat16)
        .reshape(length, heads_here, -1)
    )
    value_heads = (
        jnp.dot(all_latent, value_up, preferred_element_type=jnp.float32)
        .astype(jnp.bfloat16)
        .reshape(length, heads_here, -1)
    )
    scale = (query_plain.shape[-1] + query_turn.shape[-1]) ** (-0.5)
    key_ids = jnp.arange(length, dtype=jnp.int32)

    def one_block(items):
        index, plain_block, turn_block = items
        scores = jnp.einsum(
            "bhd,shd->hbs", plain_block, key_plain, preferred_element_type=jnp.float32
        )
        scores = (
            scores
            + jnp.einsum("bhr,sr->hbs", turn_block, all_keyturn, preferred_element_type=jnp.float32)
        ) * scale
        row_ids = index * block + jnp.arange(block, dtype=jnp.int32)
        allowed = key_ids[None, :] <= row_ids[:, None]
        scores = jnp.where(allowed[None], scores, masked_score)
        largest = jnp.max(scores, axis=-1, keepdims=True)
        powers = jnp.exp(scores - largest)
        attend = (powers / jnp.sum(powers, axis=-1, keepdims=True)).astype(jnp.bfloat16)
        return jnp.einsum(
            "hbs,shd->bhd", attend, value_heads, preferred_element_type=jnp.float32
        ).astype(jnp.bfloat16)

    attended = lax.map(
        one_block,
        (
            jnp.arange(blocks, dtype=jnp.int32),
            query_plain.reshape(blocks, block, heads_here, -1),
            query_turn.reshape(blocks, block, heads_here, -1),
        ),
    )
    attended = attended.reshape(length, heads_here, -1)
    token_heads = lax.all_to_all(attended, "sp", split_axis=0, concat_axis=1, tiled=True)
    flat_heads = token_heads.reshape(tokens_here, -1)
    head_rows = lax.all_gather(out_proj, "dp", axis=1, tiled=True)
    projected = jnp.dot(
        flat_heads,
        lax.all_gather(head_rows, "sp", axis=0, tiled=True),
        preferred_element_type=jnp.float32,
    ).astype(jnp.bfloat16)
    after_attention = resid[0].astype(jnp.float32) + projected.astype(jnp.float32)
    normed = rms_scaled(after_attention, norm_gain).astype(jnp.bfloat16)
    experts_all = sp_count * expert_gate.shape[0]
    capacity = 4 * tokens_here // experts_all
    slot_ids = assign_slots(routes[0], experts_all, capacity)
    outgoing = fill_slots(normed, slot_ids, experts_all, capacity)
    arrived = lax.all_to_all(outgoing, "sp", split_axis=0, concat_axis=0, tiled=True)
    senders, slots_now, width = arrived.shape
    rows = arrived.reshape(senders * slots_now, width)
    gate = jnp.dot(rows, expert_gate[0], preferred_element_type=jnp.float32)
    upward = jnp.dot(rows, expert_up[0], preferred_element_type=jnp.float32)
    hidden = (jax.nn.silu(gate) * upward).astype(jnp.bfloat16)
    result = jnp.dot(hidden, expert_down[0], preferred_element_type=jnp.float32).astype(
        jnp.bfloat16
    )
    returned = lax.all_to_all(
        result.reshape(senders, slots_now, width), "sp", split_axis=0, concat_axis=0, tiled=True
    )
    routed = combine_slots(returned, slot_ids, route_weight[0])
    return (after_attention + routed).astype(jnp.bfloat16)[None]


def solution(mesh):
    return jax.shard_map(
        shards,
        mesh=mesh,
        in_specs=(
            P("dp", "sp", None, None),
            P("dp", "sp", None, None),
            P("dp", "sp", None),
            P("dp", "sp", None),
            P("dp", "sp", None),
            P(),
            P(None, "sp"),
            P(None, "sp"),
            P("sp", "dp"),
            P(),
            P("sp", None, None),
            P("sp", None, None),
            P("sp", None, None),
            P("dp", "sp", None),
            P("dp", "sp", None),
        ),
        out_specs=P("dp", "sp", None),
        check_vma=False,
    )
```

profile of v0, /device:TPU:0, one launch (start us, length us, event | category | flops | bytes accessed | tf_op | source)
XLA Modules:
  0.0 489.6 jit_solution(9054582442500225814)
XLA Ops:
  12.2 16.1 %all-gather.6.cloned.1.call-done = bf16[256,2048]{1,0:T(8,128)(2,1)} async-done(((bf16[256,512]{1,0:T(8,128)(2,1)}), bf16[256,2048]{1,0:T(8,128)(2,1)}) %all-gather.6.cloned.1.call-update) | async-done | bytes 1048592 | tf_op jit(solution)/shard_map/all_gather | solution.py:146
  29.4 5.5 %all-to-all-start.1 = ((bf16[256,16,64]{0,2,1:T(8,128)(2,1)}), bf16[256,16,64]{0,2,1:T(8,128)(2,1)S(1)}, u32[]{:S(2)}, u32[]{:S(2)}) async-start(bf16[256,16,64]{0,2,1:T(8,128)(2,1)} %pad_maximum_fusion), calls=%async_computation.1 | async-start | bytes 1048576 | tf_op jit(solution)/shard_map/all_to_all | solution.py:100
  36.2 17.7 %all-to-all-done.1 = bf16[256,16,64]{0,2,1:T(8,128)(2,1)S(1)} async-done(((bf16[256,16,64]{0,2,1:T(8,128)(2,1)}), bf16[256,16,64]{0,2,1:T(8,128)(2,1)S(1)}, u32[]{:S(2)}, u32[]{:S(2)}) %all-to-all-start.1) | async-done | bytes 524320 | tf_op jit(solution)/shard_map/all_to_all | solution.py:100
  54.0 3.6 all-to-all-start
  57.6 55.9 %all_gather.13 = bf16[2048,64]{0,1:T(8,128)(2,1)S(1)} all-gather(bf16[256,64]{0,1:T(8,128)(2,1)S(1)} %pad_maximum_fusion.1), channel_id=1, replica_groups=mesh['sp'=8,'dp'=4] {'sp'}, dimensions={0}, use_global_device_ids=true | all-gather | bytes 294912 | tf_op jit(solution)/shard_map/all_gather | solution.py:96
  124.3 73.1 %while.11 = (s32[]{:T(128)}, bf16[4,512,2,128]{3,1,0,2:T(8,128)(2,1)}, s32[4]{0:T(128)S(1)}, bf16[4,512,2,128]{3,1,0,2:T(8,128)(2,1)S(1)}, bf16[2048,2,128]{2,0,...) while((s32[]{:T(128)}, ...), condition=%wide.region_4.5_spmd.clone, body=%wide.region_1.4_spmd.clone.sunk | while | flops 1360139776 | bytes 93205688 | solution.py:135
  133.3 9.1 %fusion.77 = bf16[4,512,2,128]{3,1,0,2:T(8,128)(2,1)} fusion(bf16[4,512,2,128]{3,1,0,2:T(8,128)(2,1)} %get-tuple-element.211, s32[]{:T(128)} %get-tuple-element.210, bf16[2048,2,128]{2,0,1:T(8,128)(2,1)S(1)} %copy-done.5, f32[2,512]{1,0:T(2,128)S(1)} %fusion.76, f32[2,512,2048]{2,1,0:T(8,128)} %copy-done.2), kind=kOutput, calls=%fused_computation.13.clone.1 | convolution fusion | flops 543296512 | bytes 18092544 | tf_op jit(solution)/shard_map/while/body/eval_jaxpr/hbs,shd->bhd/dot_general | solution.py:131
  151.5 9.2 %fusion.77 = bf16[4,512,2,128]{3,1,0,2:T(8,128)(2,1)} fusion(bf16[4,512,2,128]{3,1,0,2:T(8,128)(2,1)} %get-tuple-element.211, s32[]{:T(128)} %get-tuple-element.210, bf16[2048,2,128]{2,0,1:T(8,128)(2,1)S(1)} %copy-done.5, f32[2,512]{1,0:T(2,128)S(1)} %fusion.76, f32[2,512,2048]{2,1,0:T(8,128)} %copy-done.2), kind=kOutput, calls=%fused_computation.13.clone.1 | convolution fusion | flops 543296512 | bytes 18092544 | tf_op jit(solution)/shard_map/while/body/eval_jaxpr/hbs,shd->bhd/dot_general | solution.py:131
  169.8 9.1 %fusion.77 = bf16[4,512,2,128]{3,1,0,2:T(8,128)(2,1)} fusion(bf16[4,512,2,128]{3,1,0,2:T(8,128)(2,1)} %get-tuple-element.211, s32[]{:T(128)} %get-tuple-element.210, bf16[2048,2,128]{2,0,1:T(8,128)(2,1)S(1)} %copy-done.5, f32[2,512]{1,0:T(2,128)S(1)} %fusion.76, f32[2,512,2048]{2,1,0:T(8,128)} %copy-done.2), kind=kOutput, calls=%fused_computation.13.clone.1 | convolution fusion | flops 543296512 | bytes 18092544 | tf_op jit(solution)/shard_map/while/body/eval_jaxpr/hbs,shd->bhd/dot_general | solution.py:131
  188.0 9.4 %fusion.77 = bf16[4,512,2,128]{3,1,0,2:T(8,128)(2,1)} fusion(bf16[4,512,2,128]{3,1,0,2:T(8,128)(2,1)} %get-tuple-element.211, s32[]{:T(128)} %get-tuple-element.210, bf16[2048,2,128]{2,0,1:T(8,128)(2,1)S(1)} %copy-done.5, f32[2,512]{1,0:T(2,128)S(1)} %fusion.76, f32[2,512,2048]{2,1,0:T(8,128)} %copy-done.2), kind=kOutput, calls=%fused_computation.13.clone.1 | convolution fusion | flops 543296512 | bytes 18092544 | tf_op jit(solution)/shard_map/while/body/eval_jaxpr/hbs,shd->bhd/dot_general | solution.py:131
  197.3 3.7 copy.95
  201.0 3.7 all-to-all-start.2
  207.4 28.0 %all-to-all-done.2 = bf16[2048,2,128]{2,1,0:T(2,128)(2,1)S(1)} async-done(((bf16[2048,2,128]{2,1,0:T(2,128)(2,1)}), bf16[2048,2,128]{2,1,0:T(2,128)(2,1)S(1)}, u32[]{:S(2)}, u32[]{:S(2)}) %all-to-all-start.2) | async-done | bytes 1048608 | tf_op jit(solution)/shard_map/all_to_all | solution.py:144
  236.2 6.1 %multiply_reduce_fusion.1 = (f32[256]{0:T(256)S(1)}, f32[256,2048]{1,0:T(8,128)S(1)}) fusion(bf16[256,2048]{0,1:T(8,128)(2,1)S(1)} %bitcast.150, bf16[2048,2048]{1,0:T(8,128)(2,1)} %all-gather.8.cloned.1.call-done, bf16[1,256,2048]{2,1,0:T(8,128)(2,1)} %param.21), kind=kOutput, calls=%fused_computation.42 | convolution fusion | flops 2150629120 | bytes 12583936 | tf_op jit(solution)/shard_map/dot_general | solution.py:147
  242.5 6.0 %gather_fusion = bf16[1024,2048]{1,0:T(8,128)(2,1)} fusion(bf16[256,2048]{1,0:T(8,128)(2,1)S(1)} %multiply_convert_fusion.1, s32[1024]{0:T(1024)S(1)} %broadcast_clamp_fusion), kind=kCustom, calls=%fused_computation | custom fusion | bytes 8392704 | tf_op jit(solution)/shard_map/jit(_take)/gather | solution.py:55
  251.1 95.5 %all_to_all.55 = bf16[8,128,2048]{2,1,0:T(8,128)(2,1)S(1)} all-to-all(bf16[8,128,2048]{2,1,0:T(8,128)(2,1)S(1)} %select_select_fusion), channel_id=1, replica_groups=mesh['sp'=8,'dp'=4] {'sp'}, dimensions={0} | all-to-all | bytes 8388608 | tf_op jit(solution)/shard_map/all_to_all | solution.py:158
  346.6 4.5 fusion.20
  351.1 5.4 %multiply_convert_fusion = bf16[1024,1024]{1,0:T(8,128)(2,1)S(1)} fusion(f32[1024,1024]{1,0:T(8,128)S(1)} %fusion.20, bf16[1024,2048]{1,0:T(8,128)(2,1)S(1)} %bitcast.154, bf16[1,2048,1024]{2,1,0:T(8,128)(2,1)S(1)} %copy-done.10), kind=kOutput, calls=%fused_computation.31 | convolution fusion | flops 4301258752 | bytes 14680064 | tf_op jit(solution)/shard_map/dot_general | solution.py:161
  356.5 6.1 %fusion.24 = bf16[1024,2048]{1,0:T(8,128)(2,1)} fusion(bf16[1024,1024]{1,0:T(8,128)(2,1)S(1)} %multiply_convert_fusion, bf16[1,1024,2048]{2,1,0:T(8,128)(2,1)S(1)} %copy-done.11), kind=kOutput, calls=%fused_computation.34 | convolution fusion | flops 4297064448 | bytes 10485760 | tf_op jit(solution)/shard_map/dot_general | solution.py:164
  362.6 4.9 all-to-all-start.4
  368.4 91.0 %all-to-all-done.4 = bf16[8,128,2048]{2,1,0:T(8,128)(2,1)} async-done(((bf16[8,128,2048]{2,1,0:T(8,128)(2,1)}), bf16[8,128,2048]{2,1,0:T(8,128)(2,1)}, u32[]{:S(2)}, u32[]{:S(2)}) %all-to-all-start.4) | async-done | bytes 4194336 | tf_op jit(solution)/shard_map/all_to_all | solution.py:167
  459.4 8.0 %gather_fusion.1 = bf16[512,2048]{1,0:T(8,128)(2,1)} fusion(bf16[1024,2048]{1,0:T(8,128)(2,1)} %bitcast.33, s32[1024]{0:T(1024)S(1)} %pad_clamp_fusion), kind=kCustom, calls=%fused_computation.1 | custom fusion | bytes 4196352 | tf_op jit(solution)/shard_map/jit(_take)/gather | solution.py:63
  467.4 4.4 gather.15
  471.9 9.9 %multiply_reduce_fusion = f32[256,2048]{1,0:T(8,128)S(1)} fusion(bf16[256,2,2048]{2,1,0:T(2,128)(2,1)} %gather.15, pred[256,2]{1,0:T(8,128)(4,1)S(1)} %copy.102, f32[256,2]{1,0:T(8,128)S(1)} %copy.98), kind=kLoop, calls=%fused_computation.30 | loop fusion | flops 3670016 | bytes 4196864 | tf_op jit(solution)/shard_map/reduce_sum | solution.py:65
  (122 shorter events, 60.6 us)
Async XLA Ops:
  6.5 108.5 %copy-start = (bf16[256,256]{1,0:T(8,128)(2,1)S(1)}, bf16[256,256]{1,0:T(8,128)(2,1)}, u32[]{:S(2)}) copy-start(bf16[256,256]{1,0:T(8,128)(2,1)} %param.23) | copy-start | bytes 393220
  6.5 28.3 %copy-start.4 = (bf16[1,256,16,128]{3,2,1,0:T(8,128)(2,1)S(1)}, bf16[1,256,16,128]{3,2,1,0:T(8,128)(2,1)}, u32[]{:S(2)}) copy-start(bf16[1,256,16,128]{3,2,1,0:T(8,128)(2,1)} %param.17) | copy-start | bytes 3145732
  6.5 21.8 %all-gather.6.cloned.1.call-start = ((), (), s32[]{:S(2)}) async-start(), calls=%async_computation.6 | async-start | bytes 1310720 | tf_op jit(solution)/shard_map/all_gather | solution.py:146
  7.3 107.8 %all-gather.4.cloned.1.call-start = ((), (), s32[]{:S(2)}) async-start(), calls=%async_computation.5 | async-start | bytes 1179648 | tf_op jit(solution)/shard_map/all_gather | solution.py:95
  10.0 226.1 %all-gather.8.cloned.1.call-start = ((), (), s32[]{:S(2)}) async-start(), calls=%async_computation.7 | async-start | bytes 9437184 | tf_op jit(solution)/shard_map/all_gather | solution.py:149
  29.4 24.6 %all-to-all-start.1 = ((bf16[256,16,64]{0,2,1:T(8,128)(2,1)}), bf16[256,16,64]{0,2,1:T(8,128)(2,1)S(1)}, u32[]{:S(2)}, u32[]{:S(2)}) async-start(bf16[256,16,64]{0,2,1:T(8,128)(2,1)} %pad_maximum_fusion), calls=%async_computation.1 | async-start | bytes 1048576 | tf_op jit(solution)/shard_map/all_to_all | solution.py:100
  54.0 70.2 %all-to-all-start = ((bf16[256,16,128]{2,0,1:T(8,128)(2,1)}), bf16[256,16,128]{2,0,1:T(8,128)(2,1)S(1)}, u32[]{:S(2)}, u32[]{:S(2)}) async-start(bf16[256,16,128]{2,0,1:T(8,128)(2,1)} %bitcast.127), calls=%async_computation | async-start | bytes 2097152 | tf_op jit(solution)/shard_map/all_to_all | solution.py:99
  115.1 4.4 copy-start.3
  130.1 3.2 copy-start.2
  130.1 3.2 copy-start.5
  148.3 3.2 copy-start.2
  148.3 3.2 copy-start.5
  166.5 3.2 copy-start.2
  184.7 3.2 copy-start.2
  184.7 3.2 copy-start.5
  197.3 7.4 %copy-start.6 = (s32[1,256,2]{1,2,0:T(2,128)S(1)}, s32[1,256,2]{1,2,0:T(2,128)}, u32[]{:S(2)}) copy-start(s32[1,256,2]{1,2,0:T(2,128)} %param.30) | copy-start | bytes 6148
  201.0 34.4 %all-to-all-start.2 = ((bf16[2048,2,128]{2,1,0:T(2,128)(2,1)}), bf16[2048,2,128]{2,1,0:T(2,128)(2,1)S(1)}, u32[]{:S(2)}, u32[]{:S(2)}) async-start(bf16[2048,2,128]{2,1,0:T(2,128)(2,1)} %copy.95), calls=%async_computation.2 | async-start | bytes 2097152 | tf_op jit(solution)/shard_map/all_to_all | solution.py:144
  236.1 6.1 %copy-start.7 = (f32[2048]{0:T(1024)S(1)}, f32[2048]{0:T(1024)}, u32[]{:S(2)}) copy-start(f32[2048]{0:T(1024)} %param.26) | copy-start | bytes 24580
  251.1 95.5 %copy-start.9 = (bf16[1,2048,1024]{2,1,0:T(8,128)(2,1)S(1)}, bf16[1,2048,1024]{2,1,0:T(8,128)(2,1)}, u32[]{:S(2)}) copy-start(bf16[1,2048,1024]{2,1,0:T(8,128)(2,1)} %param.28) | copy-start | bytes 12582916
  346.6 4.5 copy-start.10
  351.1 5.4 %copy-start.11 = (bf16[1,1024,2048]{2,1,0:T(8,128)(2,1)S(1)}, bf16[1,1024,2048]{2,1,0:T(8,128)(2,1)}, u32[]{:S(2)}) copy-start(bf16[1,1024,2048]{2,1,0:T(8,128)(2,1)} %param.29) | copy-start | bytes 12582916
  362.6 5.6 %copy-start.8 = (f32[1,256,2]{1,2,0:T(2,128)S(1)}, f32[1,256,2]{1,2,0:T(2,128)}, u32[]{:S(2)}) copy-start(f32[1,256,2]{1,2,0:T(2,128)} %param.31) | copy-start | bytes 6148
  362.6 96.9 %all-to-all-start.4 = ((bf16[8,128,2048]{2,1,0:T(8,128)(2,1)}), bf16[8,128,2048]{2,1,0:T(8,128)(2,1)}, u32[]{:S(2)}, u32[]{:S(2)}) async-start(bf16[8,128,2048]{2,1,0:T(8,128)(2,1)} %bitcast.152), calls=%async_computation.4 | async-start | bytes 8388608 | tf_op jit(solution)/shard_map/all_to_all | solution.py:167
  467.4 15.6 %copy-start.1 = (bf16[256,256]{1,0:T(8,128)(2,1)S(1)}, bf16[256,256]{1,0:T(8,128)(2,1)}, u32[]{:S(2)}) copy-start(bf16[256,256]{1,0:T(8,128)(2,1)} %param.23) | copy-start | bytes 393220
  (1 other events, 3.2 us)
Sparse Core Ops, SparseCore 0:
  8.9 19.4 all-gather.5
  30.5 57.7 all-gather.3
  90.4 131.3 all-gather.7
where the time goes:
time: 490 us
  waiting for transfers between devices  154 us (31%)
  blocking collectives  151 us (31%)
  matrix products  80.1 us (16%)
  local copies, waits for them, and re-layouts  40 us (8%)
  other arithmetic  30.5 us (6%)
  starting transfers between devices  17.9 us (4%)
  between operations  13.5 us (3%)
    all_to_all x1, blocking collectives, shards(): lax.all_to_all(outgoing, 'sp', split_axis=0, concat_axis=0, tiled=True)  95.5 us
    all_to_all x1, waiting for transfers between devices, shards(): lax.all_to_all(result.reshape(senders, slots_now, width), 'sp', split_axi...  91 us
    all_gather x1, blocking collectives, shards(): lax.all_gather(key_turned, 'sp', axis=0, tiled=True)  55.9 us
    dot_general x4, matrix products, one_block(): jnp.einsum('hbs,shd->bhd', attend, value_heads, preferred_element_type=jn...  36.8 us
    all_to_all x1, waiting for transfers between devices, shards(): lax.all_to_all(attended, 'sp', split_axis=0, concat_axis=1, tiled=True)  28 us
    all_to_all x1, waiting for transfers between devices, shards(): lax.all_to_all(query_turned, 'sp', split_axis=1, concat_axis=0, tiled=True)  17.7 us
    all_gather x1, waiting for transfers between devices, shards(): head_rows = lax.all_gather(out_proj, 'dp', axis=1, tiled=True)  16.1 us
    gather x2, local copies, waits for them, and re-layouts, combine_slots(): jnp.take(flat_back, slot_ids, axis=0).astype(jnp.float32)  12.4 us
  transfers between devices with their start and end apart: 7, of which 4 were waited for; matrix products, arithmetic and copies ran while one was open for 18% of the time, Pallas kernels for 0%

commit v1 on v0

--- a/solution.py
+++ b/solution.py
@@ -2,6 +2,7 @@
 import jax.numpy as jnp
 from jax import lax
 from jax.sharding import PartitionSpec as P
+from jax.lax import all_to_all, axis_size
 
 epsilon = 1e-06
 rope_base = 10000.0
@@ -141,7 +142,9 @@
         ),
     )
     attended = attended.reshape(length, heads_here, -1)
-    token_heads = lax.all_to_all(attended, "sp", split_axis=0, concat_axis=1, tiled=True)
+    token_heads = jnp.concatenate(
+        all_to_all(jnp.stack(jnp.split(attended, axis_size("sp"), axis=0)), "sp", 0, 0), axis=1
+    )
     flat_heads = token_heads.reshape(tokens_here, -1)
     head_rows = lax.all_gather(out_proj, "dp", axis=1, tiled=True)
     projected = jnp.dot(

time: 490 us -> 483 us (0.986)
  waiting for transfers between devices: 154 us -> 136 us
  local copies, waits for them, and re-layouts: 40 us -> 49.2 us
    all_gather x1, waiting for transfers between devices: 16.1 us -> 0.02 us  [shards(): head_rows = lax.all_gather(out_proj, 'dp', axis=1, tiled=True)]
    unnamed x25 -> x32, local copies, waits for them, and re-layouts: 6.3 us -> 17.3 us
  transfers between devices with their start and end apart: 7 -> 7, of which waited for: 4 -> 3; matrix products, arithmetic and copies ran while one was open for 18% -> 20% of each run, Pallas kernels for 0% -> 0%
where the time goes in v1:
time: 483 us; the launch traced here: 482 us
  blocking collectives  150 us (31%)
  waiting for transfers between devices  136 us (28%)
  matrix products  80.3 us (17%)
  local copies, waits for them, and re-layouts  49.2 us (10%)
  other arithmetic  30.5 us (6%)
  starting transfers between devices  20 us (4%)
  between operations  13.5 us (3%)
    all_to_all x1, blocking collectives, shards(): lax.all_to_all(outgoing, 'sp', split_axis=0, concat_axis=0, tiled=True)  95.8 us
    all_to_all x1, waiting for transfers between devices, shards(): lax.all_to_all(result.reshape(senders, slots_now, width), 'sp', split_axi...  91.2 us
    all_gather x1, blocking collectives, shards(): lax.all_gather(key_turned, 'sp', axis=0, tiled=True)  54.6 us
    dot_general x4, matrix products, one_block(): jnp.einsum('hbs,shd->bhd', attend, value_heads, preferred_element_type=jn...  37 us
    all_to_all x1, waiting for transfers between devices, shards(): all_to_all(jnp.stack(jnp.split(attended, axis_size('sp'), axis=0)), 'sp',...  29.8 us
    unnamed x32, local copies, waits for them, and re-layouts  17.3 us
    all_to_all x1, waiting for transfers between devices, shards(): lax.all_to_all(query_turned, 'sp', split_axis=1, concat_axis=0, tiled=True)  13.1 us
    gather x2, local copies, waits for them, and re-layouts, combine_slots(): jnp.take(flat_back, slot_ids, axis=0).astype(jnp.float32)  12.4 us
  transfers between devices with their start and end apart: 7, of which 3 were waited for; matrix products, arithmetic and copies ran while one was open for 20% of the time, Pallas kernels for 0%

profile of v1, /device:TPU:0, one launch (start us, length us, event | category | flops | bytes accessed | tf_op | source)
XLA Modules:
  0.0 481.9 jit_solution(244415746128325746)
XLA Ops:
  13.2 7.3 %all-to-all-start.1 = ((bf16[256,16,64]{0,2,1:T(8,128)(2,1)}), bf16[256,16,64]{0,2,1:T(8,128)(2,1)S(1)}, u32[]{:S(2)}, u32[]{:S(2)}) async-start(bf16[256,16,64]{0,2,1:T(8,128)(2,1)} %pad_maximum_fusion), calls=%async_computation.1 | async-start | bytes 1048576 | tf_op jit(solution)/shard_map/all_to_all | solution.py:101
  21.8 13.1 %all-to-all-done.1 = bf16[256,16,64]{0,2,1:T(8,128)(2,1)S(1)} async-done(((bf16[256,16,64]{0,2,1:T(8,128)(2,1)}), bf16[256,16,64]{0,2,1:T(8,128)(2,1)S(1)}, u32[]{:S(2)}, u32[]{:S(2)}) %all-to-all-start.1) | async-done | bytes 524320 | tf_op jit(solution)/shard_map/all_to_all | solution.py:101
  35.0 3.6 all-to-all-start
  39.4 54.6 %all_gather.13 = bf16[2048,64]{0,1:T(8,128)(2,1)S(1)} all-gather(bf16[256,64]{0,1:T(8,128)(2,1)S(1)} %pad_maximum_fusion.1), channel_id=1, replica_groups=mesh['sp'=8,'dp'=4] {'sp'}, dimensions={0}, use_global_device_ids=true | all-gather | bytes 294912 | tf_op jit(solution)/shard_map/all_gather | solution.py:97
  104.6 73.8 %while.11 = (s32[]{:T(128)}, bf16[4,512,2,128]{3,1,0,2:T(8,128)(2,1)}, s32[4]{0:T(128)S(1)}, bf16[4,512,2,128]{3,1,0,2:T(8,128)(2,1)S(1)}, bf16[2048,2,128]{2,0,...) while((s32[]{:T(128)}, ...), condition=%wide.region_4.5_spmd.clone, body=%wide.region_1.4_spmd.clone.sunk | while | flops 1360139776 | bytes 93205688 | solution.py:136
  113.7 9.2 %fusion.85 = bf16[4,512,2,128]{3,1,0,2:T(8,128)(2,1)} fusion(bf16[4,512,2,128]{3,1,0,2:T(8,128)(2,1)} %get-tuple-element.195, s32[]{:T(128)} %get-tuple-element.194, bf16[2048,2,128]{2,0,1:T(8,128)(2,1)S(1)} %copy-done.5, f32[2,512]{1,0:T(2,128)S(1)} %fusion.84, f32[2,512,2048]{2,1,0:T(8,128)} %copy-done.2), kind=kOutput, calls=%fused_computation.13.clone.1 | convolution fusion | flops 543296512 | bytes 18092544 | tf_op jit(solution)/shard_map/while/body/eval_jaxpr/hbs,shd->bhd/dot_general | solution.py:132
  125.9 2.8 fusion.83
  132.4 9.6 %fusion.85 = bf16[4,512,2,128]{3,1,0,2:T(8,128)(2,1)} fusion(bf16[4,512,2,128]{3,1,0,2:T(8,128)(2,1)} %get-tuple-element.195, s32[]{:T(128)} %get-tuple-element.194, bf16[2048,2,128]{2,0,1:T(8,128)(2,1)S(1)} %copy-done.5, f32[2,512]{1,0:T(2,128)S(1)} %fusion.84, f32[2,512,2048]{2,1,0:T(8,128)} %copy-done.2), kind=kOutput, calls=%fused_computation.13.clone.1 | convolution fusion | flops 543296512 | bytes 18092544 | tf_op jit(solution)/shard_map/while/body/eval_jaxpr/hbs,shd->bhd/dot_general | solution.py:132
  151.1 9.1 %fusion.85 = bf16[4,512,2,128]{3,1,0,2:T(8,128)(2,1)} fusion(bf16[4,512,2,128]{3,1,0,2:T(8,128)(2,1)} %get-tuple-element.195, s32[]{:T(128)} %get-tuple-element.194, bf16[2048,2,128]{2,0,1:T(8,128)(2,1)S(1)} %copy-done.5, f32[2,512]{1,0:T(2,128)S(1)} %fusion.84, f32[2,512,2048]{2,1,0:T(8,128)} %copy-done.2), kind=kOutput, calls=%fused_computation.13.clone.1 | convolution fusion | flops 543296512 | bytes 18092544 | tf_op jit(solution)/shard_map/while/body/eval_jaxpr/hbs,shd->bhd/dot_general | solution.py:132
  163.3 2.8 fusion.83
  169.3 9.1 %fusion.85 = bf16[4,512,2,128]{3,1,0,2:T(8,128)(2,1)} fusion(bf16[4,512,2,128]{3,1,0,2:T(8,128)(2,1)} %get-tuple-element.195, s32[]{:T(128)} %get-tuple-element.194, bf16[2048,2,128]{2,0,1:T(8,128)(2,1)S(1)} %copy-done.5, f32[2,512]{1,0:T(2,128)S(1)} %fusion.84, f32[2,512,2048]{2,1,0:T(8,128)} %copy-done.2), kind=kOutput, calls=%fused_computation.13.clone.1 | convolution fusion | flops 543296512 | bytes 18092544 | tf_op jit(solution)/shard_map/while/body/eval_jaxpr/hbs,shd->bhd/dot_general | solution.py:132
  191.0 4.1 all-to-all-start.2
  197.7 29.8 %all-to-all-done.2 = bf16[8,256,2,128]{3,1,2,0:T(8,128)(2,1)S(1)} async-done(((bf16[8,256,2,128]{3,1,2,0:T(8,128)(2,1)}), bf16[8,256,2,128]{3,1,2,0:T(8,128)(2,1)S(1)}, u32[]{:S(2)}, u32[]{:S(2)}) %all-to-all-start.2) | async-done | bytes 1048608 | tf_op jit(solution)/shard_map/all_to_all | solution.py:146
  228.1 6.1 %multiply_reduce_fusion.1 = (f32[256]{0:T(256)S(1)}, f32[256,2048]{1,0:T(8,128)S(1)}) fusion(bf16[256,2048]{0,1:T(8,128)(2,1)S(1)} %bitcast.180, bf16[2048,2048]{1,0:T(8,128)(2,1)} %all-gather.8.cloned.1.call-done, bf16[1,256,2048]{2,1,0:T(8,128)(2,1)} %param.21), kind=kOutput, calls=%fused_computation.42 | convolution fusion | flops 2150629120 | bytes 12583936 | tf_op jit(solution)/shard_map/dot_general | solution.py:150
  234.4 6.0 %gather_fusion = bf16[1024,2048]{1,0:T(8,128)(2,1)} fusion(bf16[256,2048]{1,0:T(8,128)(2,1)S(1)} %multiply_convert_fusion.1, s32[1024]{0:T(1024)S(1)} %broadcast_clamp_fusion), kind=kCustom, calls=%fused_computation | custom fusion | bytes 8392704 | tf_op jit(solution)/shard_map/jit(_take)/gather | solution.py:56
  243.0 95.8 %all_to_all.45 = bf16[8,128,2048]{2,1,0:T(8,128)(2,1)S(1)} all-to-all(bf16[8,128,2048]{2,1,0:T(8,128)(2,1)S(1)} %select_select_fusion), channel_id=1, replica_groups=mesh['sp'=8,'dp'=4] {'sp'}, dimensions={0} | all-to-all | bytes 8388608 | tf_op jit(solution)/shard_map/all_to_all | solution.py:161
  338.8 4.5 fusion.20
  343.3 5.4 %multiply_convert_fusion = bf16[1024,1024]{1,0:T(8,128)(2,1)S(1)} fusion(f32[1024,1024]{1,0:T(8,128)S(1)} %fusion.20, bf16[1024,2048]{1,0:T(8,128)(2,1)S(1)} %bitcast.184, bf16[1,2048,1024]{2,1,0:T(8,128)(2,1)S(1)} %copy-done.10), kind=kOutput, calls=%fused_computation.31 | convolution fusion | flops 4301258752 | bytes 14680064 | tf_op jit(solution)/shard_map/dot_general | solution.py:164
  348.7 6.1 %fusion.24 = bf16[1024,2048]{1,0:T(8,128)(2,1)} fusion(bf16[1024,1024]{1,0:T(8,128)(2,1)S(1)} %multiply_convert_fusion, bf16[1,1024,2048]{2,1,0:T(8,128)(2,1)S(1)} %copy-done.11), kind=kOutput, calls=%fused_computation.34 | convolution fusion | flops 4297064448 | bytes 10485760 | tf_op jit(solution)/shard_map/dot_general | solution.py:167
  354.7 4.9 %all-to-all-start.4 = ((bf16[8,128,2048]{2,1,0:T(8,128)(2,1)}), bf16[8,128,2048]{2,1,0:T(8,128)(2,1)}, u32[]{:S(2)}, u32[]{:S(2)}) async-start(bf16[8,128,2048]{2,1,0:T(8,128)(2,1)} %bitcast.182), calls=%async_computation.4 | async-start | bytes 8388608 | tf_op jit(solution)/shard_map/all_to_all | solution.py:170
  360.6 91.2 %all-to-all-done.4 = bf16[8,128,2048]{2,1,0:T(8,128)(2,1)} async-done(((bf16[8,128,2048]{2,1,0:T(8,128)(2,1)}), bf16[8,128,2048]{2,1,0:T(8,128)(2,1)}, u32[]{:S(2)}, u32[]{:S(2)}) %all-to-all-start.4) | async-done | bytes 4194336 | tf_op jit(solution)/shard_map/all_to_all | solution.py:170
  451.8 8.0 %gather_fusion.1 = bf16[512,2048]{1,0:T(8,128)(2,1)} fusion(bf16[1024,2048]{1,0:T(8,128)(2,1)} %bitcast.40, s32[1024]{0:T(1024)S(1)} %pad_clamp_fusion), kind=kCustom, calls=%fused_computation.1 | custom fusion | bytes 4196352 | tf_op jit(solution)/shard_map/jit(_take)/gather | solution.py:64
  459.8 4.4 gather.15
  464.2 9.9 %multiply_reduce_fusion = f32[256,2048]{1,0:T(8,128)S(1)} fusion(bf16[256,2,2048]{2,1,0:T(2,128)(2,1)} %gather.15, pred[256,2]{1,0:T(8,128)(4,1)S(1)} %copy.70, f32[256,2]{1,0:T(8,128)S(1)} %copy.66), kind=kLoop, calls=%fused_computation.30 | loop fusion | flops 3670016 | bytes 4196864 | tf_op jit(solution)/shard_map/reduce_sum | solution.py:66
  (128 shorter events, 68.6 us)
Async XLA Ops:
  6.5 88.9 %copy-start = (bf16[256,256]{1,0:T(8,128)(2,1)S(1)}, bf16[256,256]{1,0:T(8,128)(2,1)}, u32[]{:S(2)}) copy-start(bf16[256,256]{1,0:T(8,128)(2,1)} %param.23) | copy-start | bytes 393220
  6.5 13.9 %copy-start.4 = (bf16[1,256,16,128]{3,2,1,0:T(8,128)(2,1)S(1)}, bf16[1,256,16,128]{3,2,1,0:T(8,128)(2,1)}, u32[]{:S(2)}) copy-start(bf16[1,256,16,128]{3,2,1,0:T(8,128)(2,1)} %param.17) | copy-start | bytes 3145732
  6.5 32.1 %all-gather.6.cloned.1.call-start = ((), (), s32[]{:S(2)}) async-start(), calls=%async_computation.6 | async-start | bytes 1310720 | tf_op jit(solution)/shard_map/all_gather | solution.py:149
  7.3 88.2 %all-gather.4.cloned.1.call-start = ((), (), s32[]{:S(2)}) async-start(), calls=%async_computation.5 | async-start | bytes 1179648 | tf_op jit(solution)/shard_map/all_gather | solution.py:96
  13.2 21.8 %all-to-all-start.1 = ((bf16[256,16,64]{0,2,1:T(8,128)(2,1)}), bf16[256,16,64]{0,2,1:T(8,128)(2,1)S(1)}, u32[]{:S(2)}, u32[]{:S(2)}) async-start(bf16[256,16,64]{0,2,1:T(8,128)(2,1)} %pad_maximum_fusion), calls=%async_computation.1 | async-start | bytes 1048576 | tf_op jit(solution)/shard_map/all_to_all | solution.py:101
  35.0 69.6 %all-to-all-start = ((bf16[256,16,128]{2,0,1:T(8,128)(2,1)}), bf16[256,16,128]{2,0,1:T(8,128)(2,1)S(1)}, u32[]{:S(2)}, u32[]{:S(2)}) async-start(bf16[256,16,128]{2,0,1:T(8,128)(2,1)} %bitcast.157), calls=%async_computation | async-start | bytes 2097152 | tf_op jit(solution)/shard_map/all_to_all | solution.py:100
  38.6 189.4 %all-gather.8.cloned.1.call-start = ((), (), s32[]{:S(2)}) async-start(), calls=%async_computation.7 | async-start | bytes 9437184 | tf_op jit(solution)/shard_map/all_gather | solution.py:152
  95.5 4.4 copy-start.3
  110.5 3.2 copy-start.2
  110.5 3.2 copy-start.5
  128.7 3.7 copy-start.2
  128.8 3.7 copy-start.5
  147.9 3.2 copy-start.2
  147.9 3.2 copy-start.5
  166.1 3.2 copy-start.2
  178.4 16.6 %copy-start.6 = (s32[1,256,2]{1,2,0:T(2,128)S(1)}, s32[1,256,2]{1,2,0:T(2,128)}, u32[]{:S(2)}) copy-start(s32[1,256,2]{1,2,0:T(2,128)} %param.30) | copy-start | bytes 6148
  191.0 36.5 %all-to-all-start.2 = ((bf16[8,256,2,128]{3,1,2,0:T(8,128)(2,1)}), bf16[8,256,2,128]{3,1,2,0:T(8,128)(2,1)S(1)}, u32[]{:S(2)}, u32[]{:S(2)}) async-start(bf16[8,256,2,128]{3,1,2,0:T(8,128)(2,1)} %fusion.36), calls=%async_computation.2 | async-start | bytes 2097152 | tf_op jit(solution)/shard_map/all_to_all | solution.py:146
  228.1 6.1 %copy-start.7 = (f32[2048]{0:T(1024)S(1)}, f32[2048]{0:T(1024)}, u32[]{:S(2)}) copy-start(f32[2048]{0:T(1024)} %param.26) | copy-start | bytes 24580
  243.0 95.8 %copy-start.9 = (bf16[1,2048,1024]{2,1,0:T(8,128)(2,1)S(1)}, bf16[1,2048,1024]{2,1,0:T(8,128)(2,1)}, u32[]{:S(2)}) copy-start(bf16[1,2048,1024]{2,1,0:T(8,128)(2,1)} %param.28) | copy-start | bytes 12582916
  338.8 4.5 copy-start.10
  343.3 5.4 %copy-start.11 = (bf16[1,1024,2048]{2,1,0:T(8,128)(2,1)S(1)}, bf16[1,1024,2048]{2,1,0:T(8,128)(2,1)}, u32[]{:S(2)}) copy-start(bf16[1,1024,2048]{2,1,0:T(8,128)(2,1)} %param.29) | copy-start | bytes 12582916
  354.7 5.6 %copy-start.8 = (f32[1,256,2]{1,2,0:T(2,128)S(1)}, f32[1,256,2]{1,2,0:T(2,128)}, u32[]{:S(2)}) copy-start(f32[1,256,2]{1,2,0:T(2,128)} %param.31) | copy-start | bytes 6148
  354.7 97.0 %all-to-all-start.4 = ((bf16[8,128,2048]{2,1,0:T(8,128)(2,1)}), bf16[8,128,2048]{2,1,0:T(8,128)(2,1)}, u32[]{:S(2)}, u32[]{:S(2)}) async-start(bf16[8,128,2048]{2,1,0:T(8,128)(2,1)} %bitcast.182), calls=%async_computation.4 | async-start | bytes 8388608 | tf_op jit(solution)/shard_map/all_to_all | solution.py:170
  459.7 15.6 %copy-start.1 = (bf16[256,256]{1,0:T(8,128)(2,1)S(1)}, bf16[256,256]{1,0:T(8,128)(2,1)}, u32[]{:S(2)}) copy-start(bf16[256,256]{1,0:T(8,128)(2,1)} %param.23) | copy-start | bytes 393220
  (1 other events, 3.2 us)
Sparse Core Ops, SparseCore 0:
  8.9 19.4 all-gather.5
  30.5 49.5 all-gather.3
  82.2 132.9 all-gather.7
